TPU v7x, 32 devices: a whole 2x2x4 slice. The times are simulated.
32 devices in a mesh: ep: 4 (over y, x), tp: 8 (over z, core).
Axes of the slice: x: 2, y: 2, z: 4, core: 2. Of those that a mesh axis runs over, the one named last changes fastest.
Arguments:
- tokens: bfloat16 [128, 2048], P(('ep', 'tp')), may hold values from -6 to 6
- lengths: int32 [128], P(('ep', 'tp')), may hold values from 64 to 1024
- cache_latent: bfloat16 [128, 1024, 512], P(('ep', 'tp')), may hold values from -6 to 6
- cache_rope_key: bfloat16 [128, 1024, 32], P(('ep', 'tp')), may hold values from -1000 to 1000
- route_ids: int32 [128, 4], P('ep'), may hold values from 0 to 31, all different within a row; in each aligned block of 32 rows (0 to 31, 32 to 63, ...) at most 8 rows name the same one
- route_weights: float32 [128, 4], P('ep'), may hold values from 0.2 to 2
- attn_gain: float32 [2048], replicated, may hold values from 0.1 to 1.9
- w_query_nope: bfloat16 [2048, 16, 64], P(None, 'tp'), may hold values from -0.125 to 0.125
- w_query_rope: bfloat16 [2048, 16, 32], P(None, 'tp'), may hold values from -0.125 to 0.125
- w_latent_down: bfloat16 [2048, 512], P(None, 'tp'), may hold values from -0.125 to 0.125
- w_key_rope: bfloat16 [2048, 32], replicated, may hold values from -0.125 to 0.125
- latent_gain: float32 [512], replicated, may hold values from 0.1 to 1.9
- w_key_up: bfloat16 [512, 16, 64], P(None, 'tp'), may hold values from -0.75 to 0.75
- w_value_up: bfloat16 [512, 16, 64], P(None, 'tp'), may hold values from -0.25 to 0.25
- w_attn_out: bfloat16 [16, 64, 2048], P('tp'), may hold values from -0.1875 to 0.1875
- ffn_gain: float32 [2048], replicated, may hold values from 0.1 to 1.9
- expert_gate: bfloat16 [32, 2048, 512], P(('ep', 'tp')), may hold values from -0.125 to 0.125
- expert_up: bfloat16 [32, 2048, 512], P(('ep', 'tp')), may hold values from -0.125 to 0.125
- expert_down: bfloat16 [32, 512, 2048], P(('ep', 'tp')), may hold values from -0.25 to 0.25
- shared_gate: bfloat16 [2048, 512], P(None, 'tp'), may hold values from -0.125 to 0.125
- shared_up: bfloat16 [2048, 512], P(None, 'tp'), may hold values from -0.125 to 0.125
- shared_down: bfloat16 [512, 2048], P('tp'), may hold values from -0.25 to 0.25
- dense_gate: bfloat16 [2048, 1024], P(None, 'tp'), may hold values from -0.125 to 0.125
- dense_up: bfloat16 [2048, 1024], P(None, 'tp'), may hold values from -0.125 to 0.125
- dense_down: bfloat16 [1024, 2048], P('tp'), may hold values from -0.1875 to 0.1875
- branch_gate: bfloat16 [2048], replicated, may hold values from -0.125 to 0.125
Outputs:
- mixed: bfloat16 [128, 2048], P(('ep', 'tp'))
- new_latent: bfloat16 [128, 512], P(('ep', 'tp'))
- new_rope_key: bfloat16 [128, 32], P(('ep', 'tp'))
Inputs may be any that keep to these rules, and one draw needn't show every extreme that they name: `route_ids`: in each aligned block of 32 rows, no expert is named by more than 8 of the block's rows, a bound that some block reaches. Each row names 4 different experts.
All inputs are finite; a program needn't handle non-finite values.
Results may differ from a plain program's by a relative error of at most 0.025.
Values may be sent and summed in bfloat16 or wider, within the bound.
A program may use at most 64 MiB of HBM per device.

v0:
```python
import jax
import jax.numpy as jnp
from jax import lax
from jax.sharding import PartitionSpec as P

epsilon = 1e-06
rope_base = 10000.0


def norm_rows(values, scales):
    values = values.astype(jnp.float32)
    factor = lax.rsqrt(jnp.mean(values * values, axis=-1, keepdims=True) + epsilon)
    return values * factor * scales


def rotate(values, positions):
    half_dim = values.shape[-1] // 2
    frequencies = rope_base ** (-jnp.arange(half_dim).astype(jnp.float32) / half_dim)
    angles = positions.astype(jnp.float32)[:, None] * frequencies[None, :]
    bcast_shape = (angles.shape[0],) + (1,) * (values.ndim - 2) + (half_dim,)
    cosine = jnp.cos(angles).reshape(bcast_shape)
    sine_val = jnp.sin(angles).reshape(bcast_shape)
    first_half = values[..., :half_dim].astype(jnp.float32)
    second_half = values[..., half_dim:].astype(jnp.float32)
    return jnp.concatenate(
        [
            first_half * cosine - second_half * sine_val,
            first_half * sine_val + second_half * cosine,
        ],
        axis=-1,
    )


def swiglu(inputs, gate_w, up_w):
    gate_val = jnp.dot(inputs, gate_w, preferred_element_type=jnp.float32)
    up_val = jnp.dot(inputs, up_w, preferred_element_type=jnp.float32)
    return (jax.nn.silu(gate_val) * up_val).astype(jnp.bfloat16)


def local(
    tokens,
    lengths,
    cache_latent,
    cache_rope_key,
    route_ids,
    route_weights,
    attn_gain,
    w_query_nope,
    w_query_rope,
    w_latent_down,
    w_key_rope,
    latent_gain,
    w_key_up,
    w_value_up,
    w_attn_out,
    ffn_gain,
    expert_gate,
    expert_up,
    expert_down,
    shared_gate,
    shared_up,
    shared_down,
    dense_gate,
    dense_up,
    dense_down,
    branch_gate,
):
    own_rows, model_width = tokens.shape
    tp_count = lax.axis_size("tp")
    ep_count = lax.axis_size("ep")
    tp_index = lax.axis_index("tp")
    local_heads = w_query_nope.shape[1]
    head_scale = (w_query_nope.shape[2] + w_query_rope.shape[2]) ** (-0.5)
    normed = norm_rows(tokens, attn_gain).astype(jnp.bfloat16)
    group_in = lax.all_gather(normed, "tp", axis=0, tiled=True)
    group_rows = group_in.shape[0]
    query_nope = jnp.dot(
        group_in, w_query_nope.reshape(model_width, -1), preferred_element_type=jnp.float32
    )
    query_nope = query_nope.astype(jnp.bfloat16).reshape(group_rows, local_heads, -1)
    query_latent = jnp.einsum(
        "ghn,rhn->ghr", query_nope, w_key_up, preferred_element_type=jnp.float32
    ).astype(jnp.bfloat16)
    query_rope = jnp.dot(
        group_in, w_query_rope.reshape(model_width, -1), preferred_element_type=jnp.float32
    )
    query_rope = query_rope.astype(jnp.bfloat16).reshape(group_rows, local_heads, -1)
    latent_part = jnp.dot(group_in, w_latent_down, preferred_element_type=jnp.float32).astype(
        jnp.bfloat16
    )
    own_latent_q, own_rope_q, latent_raw = (
        lax.all_to_all(query_latent, "tp", split_axis=0, concat_axis=1, tiled=True),
        lax.all_to_all(query_rope, "tp", split_axis=0, concat_axis=1, tiled=True),
        lax.all_to_all(latent_part, "tp", split_axis=0, concat_axis=1, tiled=True),
    )
    new_latent = norm_rows(latent_raw, latent_gain).astype(jnp.bfloat16)
    key_rope = jnp.dot(normed, w_key_rope, preferred_element_type=jnp.float32)
    new_rope = rotate(key_rope, lengths).astype(jnp.bfloat16)
    query_rot = rotate(own_rope_q, lengths).astype(jnp.bfloat16)
    scores = jnp.einsum(
        "bhr,blr->bhl", own_latent_q, cache_latent, preferred_element_type=jnp.float32
    )
    scores = scores + jnp.einsum(
        "bhe,ble->bhl", query_rot, cache_rope_key, preferred_element_type=jnp.float32
    )
    scores = scores * head_scale
    in_range = (
        jnp.arange(cache_latent.shape[1], dtype=jnp.int32)[None, None, :] < lengths[:, None, None]
    )
    scores = jnp.where(in_range, scores, -jnp.inf)
    own_score = jnp.einsum(
        "bhr,br->bh", own_latent_q, new_latent, preferred_element_type=jnp.float32
    )
    own_score = (
        own_score
        + jnp.einsum("bhe,be->bh", query_rot, new_rope, preferred_element_type=jnp.float32)
    ) * head_scale
    peak_score = jnp.maximum(jnp.max(scores, axis=-1), own_score)
    past_exp = jnp.exp(scores - peak_score[..., None])
    own_exp = jnp.exp(own_score - peak_score)
    total_exp = jnp.sum(past_exp, axis=-1) + own_exp
    past_weight = (past_exp / total_exp[..., None]).astype(jnp.bfloat16)
    own_weight = (own_exp / total_exp).astype(jnp.bfloat16)
    out_latent = jnp.einsum(
        "bhl,blr->bhr", past_weight, cache_latent, preferred_element_type=jnp.float32
    )
    out_latent = (
        out_latent
        + own_weight.astype(jnp.float32)[..., None] * new_latent.astype(jnp.float32)[:, None, :]
    )
    out_latent = out_latent.astype(jnp.bfloat16)
    head_latent = lax.all_to_all(out_latent, "tp", split_axis=1, concat_axis=0, tiled=True)
    head_values = jnp.einsum(
        "ghr,rhv->ghv", head_latent, w_value_up, preferred_element_type=jnp.float32
    ).astype(jnp.bfloat16)
    attn_part = jnp.dot(
        head_values.reshape(group_rows, -1),
        w_attn_out.reshape(-1, model_width),
        preferred_element_type=jnp.float32,
    )
    own_start = tp_index * own_rows
    placed = lax.dynamic_update_slice_in_dim(
        jnp.zeros((group_rows, model_width), jnp.float32), tokens.astype(jnp.float32), own_start, 0
    )
    group_after = lax.psum((attn_part + placed).astype(jnp.bfloat16), "tp").astype(jnp.float32)
    ffn_in = norm_rows(group_after, ffn_gain).astype(jnp.bfloat16)
    after_attn = lax.dynamic_slice_in_dim(group_after, own_start, own_rows, 0)
    shared_term = jnp.dot(
        swiglu(ffn_in, shared_gate, shared_up), shared_down, preferred_element_type=jnp.float32
    )
    branch_mix = jax.nn.sigmoid(jnp.dot(ffn_in, branch_gate, preferred_element_type=jnp.float32))
    dense_term = branch_mix[:, None] * jnp.dot(
        swiglu(ffn_in, dense_gate, dense_up), dense_down, preferred_element_type=jnp.float32
    )
    top_count = route_ids.shape[1]
    expert_local = expert_gate.shape[0]
    capacity = max(
        2, (2 * own_rows * top_count + expert_local * ep_count - 1) // (expert_local * ep_count)
    )
    target_count = ep_count * expert_local
    slot_count = target_count * capacity
    column = route_ids // expert_local % tp_count
    target = route_ids // (expert_local * tp_count) * expert_local + route_ids % expert_local
    flat_target = jnp.where(column == tp_index, target, -1).reshape(-1)
    target_hits = (
        flat_target[:, None] == jnp.arange(target_count, dtype=jnp.int32)[None, :]
    ).astype(jnp.int32)
    earlier = jnp.cumsum(target_hits, axis=0) - target_hits
    rank_in = jnp.sum(earlier * target_hits, axis=1)
    slot_index = jnp.where(flat_target >= 0, flat_target * capacity + rank_in, -1).reshape(
        group_rows, top_count
    )
    slot_match = slot_index[:, :, None] == jnp.arange(slot_count, dtype=jnp.int32)[None, None, :]
    dispatch = jnp.any(slot_match, axis=1).astype(jnp.bfloat16)
    combine = jnp.sum(jnp.where(slot_match, route_weights[:, :, None], 0.0), axis=1)
    outgoing = jnp.einsum("gs,gd->sd", dispatch, ffn_in, preferred_element_type=jnp.float32).astype(
        jnp.bfloat16
    )
    outgoing = outgoing.reshape(ep_count, expert_local, capacity, model_width)
    arrived = lax.all_to_all(outgoing, "ep", split_axis=0, concat_axis=0, tiled=True)
    gate_val = jnp.einsum(
        "sxcd,xdf->sxcf", arrived, expert_gate, preferred_element_type=jnp.float32
    )
    up_val = jnp.einsum("sxcd,xdf->sxcf", arrived, expert_up, preferred_element_type=jnp.float32)
    act_val = (jax.nn.silu(gate_val) * up_val).astype(jnp.bfloat16)
    result = jnp.einsum(
        "sxcf,xfd->sxcd", act_val, expert_down, preferred_element_type=jnp.float32
    ).astype(jnp.bfloat16)
    returned = lax.all_to_all(result, "ep", split_axis=0, concat_axis=0, tiled=True)
    routed = jnp.dot(
        combine,
        returned.reshape(slot_count, model_width).astype(jnp.float32),
        precision=lax.Precision.HIGHEST,
    )
    ffn_total = routed + shared_term + dense_term
    mixed = (
        after_attn
        + lax.psum_scatter(
            ffn_total.astype(jnp.bfloat16), "tp", scatter_dimension=0, tiled=True
        ).astype(jnp.float32)
    ).astype(jnp.bfloat16)
    return (mixed, new_latent, new_rope)


def solution(mesh):
    in_specs = (
        P(("ep", "tp"), None),
        P(("ep", "tp")),
        P(("ep", "tp"), None, None),
        P(("ep", "tp"), None, None),
        P("ep", None),
        P("ep", None),
        P(),
        P(None, "tp", None),
        P(None, "tp", None),
        P(None, "tp"),
        P(),
        P(),
        P(None, "tp", None),
        P(None, "tp", None),
        P("tp", None, None),
        P(),
        P(("ep", "tp"), None, None),
        P(("ep", "tp"), None, None),
        P(("ep", "tp"), None, None),
        P(None, "tp"),
        P(None, "tp"),
        P("tp", None),
        P(None, "tp"),
        P(None, "tp"),
        P("tp", None),
        P(),
    )
    out_specs = (P(("ep", "tp"), None), P(("ep", "tp"), None), P(("ep", "tp"), None))
    return jax.shard_map(local, mesh=mesh, in_specs=in_specs, out_specs=out_specs, check_vma=False)
```

profile of v0, /device:TPU:0, one launch (start us, length us, event | category | flops | bytes accessed | tf_op | source)
XLA Modules:
  0.0 222.2 jit_solution(12282794214563576408)
XLA Ops:
  7.2 1.0 fusion.58
  8.2 0.8 fusion.95
  9.1 15.7 %all-gather = bf16[8,4,2048]{2,1,0:T(4,128)(2,1)S(1)} all-gather(bf16[1,4,2048]{2,1,0:T(4,128)(2,1)S(1)} %fusion.95), channel_id=1, replica_groups=mesh['ep'=4,'tp'=8] {'tp'}, dimensions={0}, use_global_device_ids=true | all-gather | bytes 147456 | tf_op jit(solution)/shard_map/all_gather | solution.py:75
  24.8 1.1 convolution_convert_fusion.5
  26.7 4.6 %all-to-all-start.2 = ((bf16[8,2,128]{2,1,0:T(2,128)(2,1)}), bf16[8,2,128]{2,1,0:T(2,128)(2,1)S(1)}, u32[]{:S(2)}, u32[]{:S(2)}) async-start(bf16[8,2,128]{2,1,0:T(2,128)(2,1)} %reshape.224), calls=%async_computation.2 | async-start | bytes 8192 | tf_op jit(solution)/shard_map/all_to_all | solution.py:94
  32.7 1.1 fusion.93
  35.3 1.1 convolution_convert_fusion.6
  36.4 1.3 convolution_convert_fusion.4
  41.6 5.1 %all-to-all-start.1 = ((bf16[8,2,128]{2,1,0:T(2,128)(2,1)}), bf16[8,2,128]{2,1,0:T(2,128)(2,1)S(1)}, u32[]{:S(2)}, u32[]{:S(2)}) async-start(bf16[8,2,128]{2,1,0:T(2,128)(2,1)} %reshape.222), calls=%async_computation.1 | async-start | bytes 8192 | tf_op jit(solution)/shard_map/all_to_all | solution.py:93
  47.0 5.2 %all-to-all-done.1 = bf16[8,2,128]{2,1,0:T(2,128)(2,1)S(1)} async-done(((bf16[8,2,128]{2,1,0:T(2,128)(2,1)}), bf16[8,2,128]{2,1,0:T(2,128)(2,1)S(1)}, u32[]{:S(2)}, u32[]{:S(2)}) %all-to-all-start.1) | async-done | bytes 4128 | tf_op jit(solution)/shard_map/all_to_all | solution.py:93
  52.2 3.3 %all-to-all-start = ((bf16[32,2,512]{2,1,0:T(2,128)(2,1)}), bf16[32,2,512]{2,1,0:T(2,128)(2,1)S(1)}, u32[]{:S(2)}, u32[]{:S(2)}) async-start(bf16[32,2,512]{2,1,0:T(2,128)(2,1)} %copy.64), calls=%async_computation | async-start | bytes 131072 | tf_op jit(solution)/shard_map/all_to_all | solution.py:92
  56.0 5.4 %all-to-all-done = bf16[32,2,512]{2,1,0:T(2,128)(2,1)S(1)} async-done(((bf16[32,2,512]{2,1,0:T(2,128)(2,1)}), bf16[32,2,512]{2,1,0:T(2,128)(2,1)S(1)}, u32[]{:S(2)}, u32[]{:S(2)}) %all-to-all-start) | async-done | bytes 65568 | tf_op jit(solution)/shard_map/all_to_all | solution.py:92
  61.7 3.5 %fusion.100 = f32[4,16,1024]{2,1,0:T(8,128)S(1)} fusion(bf16[4,16,512]{2,1,0:T(8,128)(2,1)S(1)} %all_to_all.58, bf16[4,1024,512]{2,1,0:T(8,128)(2,1)} %param.28), kind=kOutput, calls=%fused_computation.141 | convolution fusion | flops 67108864 | bytes 4521984 | tf_op jit(solution)/shard_map/bhr,blr->bhl/dot_general | solution.py:100
  67.2 3.3 %all-to-all-start.3 = ((bf16[4,16,512]{2,0,1:T(4,128)(2,1)}), bf16[4,16,512]{2,0,1:T(4,128)(2,1)S(1)}, u32[]{:S(2)}, u32[]{:S(2)}) async-start(bf16[4,16,512]{2,0,1:T(4,128)(2,1)} %copy.68), calls=%async_computation.3 | async-start | bytes 131072 | tf_op jit(solution)/shard_map/all_to_all | solution.py:132
  71.3 5.1 %all-to-all-done.3 = bf16[4,16,512]{2,0,1:T(4,128)(2,1)S(1)} async-done(((bf16[4,16,512]{2,0,1:T(4,128)(2,1)}), bf16[4,16,512]{2,0,1:T(4,128)(2,1)S(1)}, u32[]{:S(2)}, u32[]{:S(2)}) %all-to-all-start.3) | async-done | bytes 65568 | tf_op jit(solution)/shard_map/all_to_all | solution.py:132
  76.5 1.3 convolution_bitcast_fusion
  78.6 53.5 %all-reduce.4.cloned.1.call-done = bf16[32,2048]{1,0:T(8,128)(2,1)} async-done(((bf16[32,2048]{1,0:T(8,128)(2,1)}), bf16[32,2048]{1,0:T(8,128)(2,1)}) %all-reduce.4.cloned.1.call-update) | async-done | bytes 131088 | tf_op jit(solution)/shard_map/psum | solution.py:145
  132.1 1.0 multiply_reduce_fusion
  133.2 1.8 fusion.2
  135.0 3.6 %all-to-all-start.4 = ((bf16[4,1,8,2048]{3,2,1,0:T(8,128)(2,1)}), bf16[4,1,8,2048]{3,2,1,0:T(8,128)(2,1)S(1)}, u32[]{:S(2)}, u32[]{:S(2)}) async-start(bf16[4,1,8,2048]{3,2,1,0:T(8,128)(2,1)} %fusion.2), calls=%async_computation.4 | async-start | bytes 262144 | tf_op jit(solution)/shard_map/all_to_all | solution.py:180
  138.6 1.8 fusion.96
  140.4 1.9 fusion.97
  142.3 1.4 all-to-all-done.4
  143.7 2.0 fusion.13
  145.7 3.2 %fusion.3 = bf16[4,1,8,2048]{3,2,1,0:T(8,128)(2,1)} fusion(bf16[1,512,2048]{2,1,0:T(8,128)(2,1)S(1)} %copy-done, bf16[1,2048,512]{2,1,0:T(8,128)(2,1)} %param.43, bf16[4,1,8,2048]{3,2,1,0:T(8,128)(2,1)S(1)} %all-to-all-done.4, f32[4,1,8,512]{3,2,0,1:T(8,128)S(1)} %fusion.13), kind=kOutput, calls=%fused_computation.8 | convolution fusion | flops 134381568 | bytes 4521984 | tf_op jit(solution)/shard_map/sxcf,xfd->sxcd/dot_general | solution.py:186
  148.9 3.5 %all-to-all-start.5 = ((bf16[4,1,8,2048]{3,2,1,0:T(8,128)(2,1)}), bf16[4,1,8,2048]{3,2,1,0:T(8,128)(2,1)S(1)}, u32[]{:S(2)}, u32[]{:S(2)}) async-start(bf16[4,1,8,2048]{3,2,1,0:T(8,128)(2,1)} %fusion.3), calls=%async_computation.5 | async-start | bytes 262144 | tf_op jit(solution)/shard_map/all_to_all | solution.py:189
  153.2 4.2 %all-to-all-done.5 = bf16[4,1,8,2048]{3,2,1,0:T(8,128)(2,1)S(1)} async-done(((bf16[4,1,8,2048]{3,2,1,0:T(8,128)(2,1)}), bf16[4,1,8,2048]{3,2,1,0:T(8,128)(2,1)S(1)}, u32[]{:S(2)}, u32[]{:S(2)}) %all-to-all-start.5) | async-done | bytes 131104 | tf_op jit(solution)/shard_map/all_to_all | solution.py:189
  157.6 1.4 convolution_add_fusion
  159.1 2.2 fusion.1
  161.3 1.3 pad_maximum_fusion.3
  162.6 51.4 %all-reduce.6.cloned.1.call-done = bf16[32,2048]{1,0:T(8,128)(2,1)} async-done(((bf16[32,2048]{1,0:T(8,128)(2,1)}), bf16[32,2048]{1,0:T(8,128)(2,1)}) %all-reduce.6.cloned.1.call-update) | async-done | bytes 131088
  214.0 1.4 add_convert_fusion
  (96 shorter events, 12.4 us)
Async XLA Ops:
  7.2 138.5 %copy-start = (bf16[1,512,2048]{2,1,0:T(8,128)(2,1)S(1)}, bf16[1,512,2048]{2,1,0:T(8,128)(2,1)}, u32[]{:S(2)}) copy-start(bf16[1,512,2048]{2,1,0:T(8,128)(2,1)} %param.44) | copy-start | bytes 6291460
  7.2 33.2 %copy-start.18 = (u32[32]{0:T(128)S(1)}, u32[32]{0:T(128)}, u32[]{:S(2)}) copy-start(u32[32]{0:T(128)} %constant.109) | copy-start | bytes 388
  7.2 30.7 %copy-start.10 = (bf16[512,2,64]{0,2,1:T(8,128)(2,1)S(1)}, bf16[512,2,64]{0,2,1:T(8,128)(2,1)}, u32[]{:S(2)}) copy-start(bf16[512,2,64]{0,2,1:T(8,128)(2,1)} %param.38) | copy-start | bytes 393220
  7.2 31.0 %copy-start.14 = (bf16[2048]{0:T(1024)(128)(2,1)S(1)}, bf16[2048]{0:T(1024)(128)(2,1)}, u32[]{:S(2)}) copy-start(bf16[2048]{0:T(1024)(128)(2,1)} %param.51) | copy-start | bytes 12292
  7.2 48.5 %copy-start.16 = (f32[512]{0:T(512)S(1)}, f32[512]{0:T(512)}, u32[]{:S(2)}) copy-start(f32[512]{0:T(512)} %param.37) | copy-start | bytes 6148
  26.7 14.9 %all-to-all-start.2 = ((bf16[8,2,128]{2,1,0:T(2,128)(2,1)}), bf16[8,2,128]{2,1,0:T(2,128)(2,1)S(1)}, u32[]{:S(2)}, u32[]{:S(2)}) async-start(bf16[8,2,128]{2,1,0:T(2,128)(2,1)} %reshape.224), calls=%async_computation.2 | async-start | bytes 8192 | tf_op jit(solution)/shard_map/all_to_all | solution.py:94
  38.1 23.3 %copy-start.12 = (bf16[4,16]{1,0:T(4,128)(2,1)}, bf16[4,16]{1,0:T(4,128)(2,1)S(1)}, u32[]{:S(2)}) copy-start(bf16[4,16]{1,0:T(4,128)(2,1)S(1)} %get-tuple-element.10) | copy-start | bytes 388
  41.6 10.6 %all-to-all-start.1 = ((bf16[8,2,128]{2,1,0:T(2,128)(2,1)}), bf16[8,2,128]{2,1,0:T(2,128)(2,1)S(1)}, u32[]{:S(2)}, u32[]{:S(2)}) async-start(bf16[8,2,128]{2,1,0:T(2,128)(2,1)} %reshape.222), calls=%async_computation.1 | async-start | bytes 8192 | tf_op jit(solution)/shard_map/all_to_all | solution.py:93
  52.2 9.2 %all-to-all-start = ((bf16[32,2,512]{2,1,0:T(2,128)(2,1)}), bf16[32,2,512]{2,1,0:T(2,128)(2,1)S(1)}, u32[]{:S(2)}, u32[]{:S(2)}) async-start(bf16[32,2,512]{2,1,0:T(2,128)(2,1)} %copy.64), calls=%async_computation | async-start | bytes 131072 | tf_op jit(solution)/shard_map/all_to_all | solution.py:92
  55.8 9.4 %copy-start.15 = (bf16[4,512]{1,0:T(4,128)(2,1)}, bf16[4,512]{1,0:T(4,128)(2,1)S(1)}, u32[]{:S(2)}) copy-start(bf16[4,512]{1,0:T(4,128)(2,1)S(1)} %get-tuple-element.4) | copy-start | bytes 12292
  61.6 3.5 %copy-start.6 = (bf16[4,1024,32]{1,2,0:T(8,128)(2,1)S(1)}, bf16[4,1024,32]{1,2,0:T(8,128)(2,1)}, u32[]{:S(2)}) copy-start(bf16[4,1024,32]{1,2,0:T(8,128)(2,1)} %param.29) | copy-start | bytes 786436
  61.6 4.1 %copy-start.1 = (bf16[4,1024,512]{2,1,0:T(8,128)(2,1)S(1)}, bf16[4,1024,512]{2,1,0:T(8,128)(2,1)}, u32[]{:S(2)}) copy-start(bf16[4,1024,512]{2,1,0:T(8,128)(2,1)} %param.28) | copy-start | bytes 12582916
  65.8 4.8 %copy-start.17 = (f32[32,4]{0,1:T(4,128)S(1)}, f32[32,4]{0,1:T(4,128)}, u32[]{:S(2)}) copy-start(f32[32,4]{0,1:T(4,128)} %param.31) | copy-start | bytes 1540
  65.8 10.7 %copy-start.4 = (bf16[2,64,2048]{2,1,0:T(8,128)(2,1)S(1)}, bf16[2,64,2048]{2,1,0:T(8,128)(2,1)}, u32[]{:S(2)}) copy-start(bf16[2,64,2048]{2,1,0:T(8,128)(2,1)} %param.40) | copy-start | bytes 1572868
  65.8 12.0 %copy-start.9 = (bf16[4,2048]{1,0:T(4,128)(2,1)S(1)}, bf16[4,2048]{1,0:T(4,128)(2,1)}, u32[]{:S(2)}) copy-start(bf16[4,2048]{1,0:T(4,128)(2,1)} %param.26) | copy-start | bytes 49156
  66.5 66.7 %copy-start.8 = (f32[2048]{0:T(1024)S(1)}, f32[2048]{0:T(1024)}, u32[]{:S(2)}) copy-start(f32[2048]{0:T(1024)} %param.41) | copy-start | bytes 24580
  66.5 72.1 %copy-start.3 = (bf16[2048,128]{1,0:T(8,128)(2,1)S(1)}, bf16[2048,128]{1,0:T(8,128)(2,1)}, u32[]{:S(2)}) copy-start(bf16[2048,128]{1,0:T(8,128)(2,1)} %param.48) | copy-start | bytes 1572868
  67.2 9.2 %all-to-all-start.3 = ((bf16[4,16,512]{2,0,1:T(4,128)(2,1)}), bf16[4,16,512]{2,0,1:T(4,128)(2,1)S(1)}, u32[]{:S(2)}, u32[]{:S(2)}) async-start(bf16[4,16,512]{2,0,1:T(4,128)(2,1)} %copy.68), calls=%async_computation.3 | async-start | bytes 131072 | tf_op jit(solution)/shard_map/all_to_all | solution.py:132
  70.5 61.6 %all-reduce.4.cloned.1.call-start = ((), (), s32[]{:S(2)}) async-start(), calls=%async_computation.6 | async-start | bytes 262144 | tf_op jit(solution)/shard_map/psum | solution.py:145
  135.0 8.7 %all-to-all-start.4 = ((bf16[4,1,8,2048]{3,2,1,0:T(8,128)(2,1)}), bf16[4,1,8,2048]{3,2,1,0:T(8,128)(2,1)S(1)}, u32[]{:S(2)}, u32[]{:S(2)}) async-start(bf16[4,1,8,2048]{3,2,1,0:T(8,128)(2,1)} %fusion.2), calls=%async_computation.4 | async-start | bytes 262144 | tf_op jit(solution)/shard_map/all_to_all | solution.py:180
  145.7 6.7 %copy-start.2 = (bf16[32,2048]{1,0:T(8,128)(2,1)S(1)}, bf16[32,2048]{1,0:T(8,128)(2,1)}, u32[]{:S(2)}) copy-start(bf16[32,2048]{1,0:T(8,128)(2,1)} %all-reduce.4.cloned.1.call-done) | copy-start | bytes 393220
  145.7 6.7 %copy-start.13 = (bf16[2048,1]{0,1:T(2,128)(2,1)S(1)}, bf16[2048,1]{0,1:T(2,128)(2,1)}, u32[]{:S(2)}) copy-start(bf16[2048,1]{0,1:T(2,128)(2,1)} %reshape.219) | copy-start | bytes 12292
  145.7 11.7 %copy-start.11 = (f32[32,32]{1,0:T(8,128)S(1)}, f32[32,32]{1,0:T(8,128)}, u32[]{:S(2)}) copy-start(f32[32,32]{1,0:T(8,128)} %select_reduce_fusion) | copy-start | bytes 12292
  145.7 11.9 %copy-start.7 = (bf16[64,2048]{1,0:T(8,128)(2,1)S(1)}, bf16[64,2048]{1,0:T(8,128)(2,1)}, u32[]{:S(2)}) copy-start(bf16[64,2048]{1,0:T(8,128)(2,1)} %param.47) | copy-start | bytes 786436
  148.9 10.2 %copy-start.5 = (bf16[128,2048]{1,0:T(8,128)(2,1)S(1)}, bf16[128,2048]{1,0:T(8,128)(2,1)}, u32[]{:S(2)}) copy-start(bf16[128,2048]{1,0:T(8,128)(2,1)} %param.50) | copy-start | bytes 1572868
  148.9 8.4 %all-to-all-start.5 = ((bf16[4,1,8,2048]{3,2,1,0:T(8,128)(2,1)}), bf16[4,1,8,2048]{3,2,1,0:T(8,128)(2,1)S(1)}, u32[]{:S(2)}, u32[]{:S(2)}) async-start(bf16[4,1,8,2048]{3,2,1,0:T(8,128)(2,1)} %fusion.3), calls=%async_computation.5 | async-start | bytes 262144 | tf_op jit(solution)/shard_map/all_to_all | solution.py:189
  152.4 61.6 %all-reduce.6.cloned.1.call-start = ((), (), s32[]{:S(2)}) async-start(), calls=%async_computation.7 | async-start | bytes 262144
Sparse Core Ops, SparseCore 0:
  78.6 53.4 all-reduce.3
  161.4 52.5 all-reduce.5
where the time goes:
time: 223 us; the launch traced here: 222 us
  waiting for transfers between devices  126 us (57%)
  matrix products  26.3 us (12%)
  starting transfers between devices  23.6 us (11%)
  blocking collectives  15.7 us (7%)
  between operations  15.1 us (7%)
  other arithmetic  9.66 us (4%)
  local copies, waits for them, and re-layouts  5.69 us (3%)
    psum x1, waiting for transfers between devices, local(): lax.psum((attn_part + placed).astype(jnp.bfloat16), 'tp')  53.5 us
    unnamed x3, waiting for transfers between devices  51.4 us
    all_gather x1, blocking collectives, local(): group_in = lax.all_gather(normed, 'tp', axis=0, tiled=True)  15.7 us
    all_to_all x1, waiting for transfers between devices, local(): lax.all_to_all(query_latent, 'tp', split_axis=0, concat_axis=1, tiled=True)  5.38 us
    all_to_all x1, waiting for transfers between devices, local(): lax.all_to_all(query_rope, 'tp', split_axis=0, concat_axis=1, tiled=True)  5.2 us
    all_to_all x1, starting transfers between devices, local(): lax.all_to_all(query_rope, 'tp', split_axis=0, concat_axis=1, tiled=True)  5.11 us
    all_to_all x1, waiting for transfers between devices, local(): lax.all_to_all(out_latent, 'tp', split_axis=1, concat_axis=0, tiled=True)  5.08 us
    all_to_all x1, starting transfers between devices, local(): lax.all_to_all(latent_part, 'tp', split_axis=0, concat_axis=1, tiled=True)  4.6 us
  transfers between devices with their start and end apart: 8, of which 7 were waited for; matrix products, arithmetic and copies ran while one was open for 8% of the time, Pallas kernels for 0%

commit v1 on v0

--- a/solution.py
+++ b/solution.py
@@ -72,7 +72,22 @@
     local_heads = w_query_nope.shape[1]
     head_scale = (w_query_nope.shape[2] + w_query_rope.shape[2]) ** (-0.5)
     normed = norm_rows(tokens, attn_gain).astype(jnp.bfloat16)
-    group_in = lax.all_gather(normed, "tp", axis=0, tiled=True)
+
+    def cover_the_outputs(payload):
+        bus_axis = "tp"
+        shares = lax.axis_size(bus_axis)
+        low = sorted(((i, (i + 1) % shares) for i in range(shares)))
+        current_value = payload
+        sheets = [current_value]
+        s = 1
+        while s < shares:
+            current_value = lax.ppermute(current_value, bus_axis, low)
+            sheets.insert(0, current_value)
+            s = s + 1
+        e_next = jnp.concatenate(sheets, 0)
+        return jnp.roll(e_next, (lax.axis_index(bus_axis) + 1) * payload.shape[0], 0)
+
+    group_in = cover_the_outputs(normed)
     group_rows = group_in.shape[0]
     query_nope = jnp.dot(
         group_in, w_query_nope.reshape(model_width, -1), preferred_element_type=jnp.float32

time: 223 us -> 237 us (1.063)
  waiting for transfers between devices: 126 us -> 158 us
  blocking collectives: 15.7 us -> 0 us
  starting transfers between devices: 23.6 us -> 21.1 us
    ppermute x0 -> x7, waiting for transfers between devices: none -> 27.8 us  [cover_the_outputs(): current_value = lax.ppermute(current_value, bus_axis, low)]
    all_gather x1 -> x0, blocking collectives: 15.7 us -> none  [local(): group_in = lax.all_gather(normed, 'tp', axis=0, tiled=True)]
    all_to_all x1, waiting for transfers between devices: 0.01 us -> 3.83 us  [local(): lax.all_to_all(latent_part, 'tp', split_axis=0, concat_axis=1, tiled=True)]
    unnamed x46 -> x43, local copies, waits for them, and re-layouts: 3.64 us -> 4.95 us
  transfers between devices with their start and end apart: 8 -> 15, of which waited for: 7 -> 15; matrix products, arithmetic and copies ran while one was open for 8% -> 7% of each run, Pallas kernels for 0% -> 0%
where the time goes in v1:
time: 237 us; the launch traced here: 236 us
  waiting for transfers between devices  158 us (67%)
  matrix products  25.2 us (11%)
  starting transfers between devices  21.1 us (9%)
  between operations  15.1 us (6%)
  other arithmetic  9.59 us (4%)
  local copies, waits for them, and re-layouts  7.24 us (3%)
    psum x1, waiting for transfers between devices, local(): lax.psum((attn_part + placed).astype(jnp.bfloat16), 'tp')  54 us
    unnamed x3, waiting for transfers between devices  51.4 us
    ppermute x7, waiting for transfers between devices, cover_the_outputs(): current_value = lax.ppermute(current_value, bus_axis, low)  27.8 us
    all_to_all x1, waiting for transfers between devices, local(): lax.all_to_all(query_latent, 'tp', split_axis=0, concat_axis=1, tiled=True)  5.38 us
    all_to_all x1, waiting for transfers between devices, local(): lax.all_to_all(query_rope, 'tp', split_axis=0, concat_axis=1, tiled=True)  5.13 us
    all_to_all x1, waiting for transfers between devices, local(): lax.all_to_all(out_latent, 'tp', split_axis=1, concat_axis=0, tiled=True)  5.08 us
    unnamed x43, local copies, waits for them, and re-layouts  4.95 us
  transfers between devices with their start and end apart: 15, of which 15 were waited for; matrix products, arithmetic and copies ran while one was open for 7% of the time, Pallas kernels for 0%

profile of v1, /device:TPU:0, one launch (start us, length us, event | category | flops | bytes accessed | tf_op | source)
XLA Modules:
  0.0 236.4 jit_solution(13082891619374500317)
XLA Ops:
  11.8 3.2 %collective-permute-done = bf16[4,2048]{1,0:T(4,128)(2,1)S(1)} collective-permute-done((bf16[4,2048]{1,0:T(4,128)(2,1)S(1)}, bf16[4,2048]{1,0:T(4,128)(2,1)S(1)}, u32[]{:S(2)}, u32[]{:S(2)}) %collective-permute-start) | collective-permute-done | bytes 16416 | tf_op jit(solution)/shard_map/ppermute | solution.py:84
  15.3 4.7 %collective-permute-done.1 = bf16[4,2048]{1,0:T(4,128)(2,1)S(1)} collective-permute-done((bf16[4,2048]{1,0:T(4,128)(2,1)S(1)}, bf16[4,2048]{1,0:T(4,128)(2,1)S(1)}, u32[]{:S(2)}, u32[]{:S(2)}) %collective-permute-start.1) | collective-permute-done | bytes 16416 | tf_op jit(solution)/shard_map/ppermute | solution.py:84
  20.0 4.9 %collective-permute-done.2 = bf16[4,2048]{1,0:T(4,128)(2,1)S(1)} collective-permute-done((bf16[4,2048]{1,0:T(4,128)(2,1)S(1)}, bf16[4,2048]{1,0:T(4,128)(2,1)S(1)}, u32[]{:S(2)}, u32[]{:S(2)}) %collective-permute-start.2) | collective-permute-done | bytes 16416 | tf_op jit(solution)/shard_map/ppermute | solution.py:84
  25.6 4.3 %collective-permute-done.3 = bf16[4,2048]{1,0:T(4,128)(2,1)S(1)} collective-permute-done((bf16[4,2048]{1,0:T(4,128)(2,1)S(1)}, bf16[4,2048]{1,0:T(4,128)(2,1)S(1)}, u32[]{:S(2)}, u32[]{:S(2)}) %collective-permute-start.3) | collective-permute-done | bytes 16416 | tf_op jit(solution)/shard_map/ppermute | solution.py:84
  30.0 4.8 %collective-permute-done.4 = bf16[4,2048]{1,0:T(4,128)(2,1)S(1)} collective-permute-done((bf16[4,2048]{1,0:T(4,128)(2,1)S(1)}, bf16[4,2048]{1,0:T(4,128)(2,1)S(1)}, u32[]{:S(2)}, u32[]{:S(2)}) %collective-permute-start.4) | collective-permute-done | bytes 16416 | tf_op jit(solution)/shard_map/ppermute | solution.py:84
  35.6 4.2 %collective-permute-done.5 = bf16[4,2048]{1,0:T(4,128)(2,1)S(1)} collective-permute-done((bf16[4,2048]{1,0:T(4,128)(2,1)S(1)}, bf16[4,2048]{1,0:T(4,128)(2,1)S(1)}, u32[]{:S(2)}, u32[]{:S(2)}) %collective-permute-start.5) | collective-permute-done | bytes 16416 | tf_op jit(solution)/shard_map/ppermute | solution.py:84
  39.9 1.3 reshape.217
  43.2 1.6 collective-permute-done.6
  48.4 3.3 %all-to-all-start.2 = ((bf16[8,2,128]{2,1,0:T(2,128)(2,1)}), bf16[8,2,128]{2,1,0:T(2,128)(2,1)S(1)}, u32[]{:S(2)}, u32[]{:S(2)}) async-start(bf16[8,2,128]{2,1,0:T(2,128)(2,1)} %reshape.222), calls=%async_computation.2 | async-start | bytes 8192 | tf_op jit(solution)/shard_map/all_to_all | solution.py:109
  53.4 3.8 %all-to-all-done.2 = bf16[8,2,128]{2,1,0:T(2,128)(2,1)S(1)} async-done(((bf16[8,2,128]{2,1,0:T(2,128)(2,1)}), bf16[8,2,128]{2,1,0:T(2,128)(2,1)S(1)}, u32[]{:S(2)}, u32[]{:S(2)}) %all-to-all-start.2) | async-done | bytes 4128 | tf_op jit(solution)/shard_map/all_to_all | solution.py:109
  57.2 3.3 %all-to-all-start.1 = ((bf16[8,2,128]{2,1,0:T(2,128)(2,1)}), bf16[8,2,128]{2,1,0:T(2,128)(2,1)S(1)}, u32[]{:S(2)}, u32[]{:S(2)}) async-start(bf16[8,2,128]{2,1,0:T(2,128)(2,1)} %reshape.220), calls=%async_computation.1 | async-start | bytes 8192 | tf_op jit(solution)/shard_map/all_to_all | solution.py:108
  60.9 5.1 %all-to-all-done.1 = bf16[8,2,128]{2,1,0:T(2,128)(2,1)S(1)} async-done(((bf16[8,2,128]{2,1,0:T(2,128)(2,1)}), bf16[8,2,128]{2,1,0:T(2,128)(2,1)S(1)}, u32[]{:S(2)}, u32[]{:S(2)}) %all-to-all-start.1) | async-done | bytes 4128 | tf_op jit(solution)/shard_map/all_to_all | solution.py:108
  66.0 3.3 %all-to-all-start = ((bf16[32,2,512]{2,1,0:T(2,128)(2,1)}), bf16[32,2,512]{2,1,0:T(2,128)(2,1)S(1)}, u32[]{:S(2)}, u32[]{:S(2)}) async-start(bf16[32,2,512]{2,1,0:T(2,128)(2,1)} %copy.64), calls=%async_computation | async-start | bytes 131072 | tf_op jit(solution)/shard_map/all_to_all | solution.py:107
  69.8 5.4 %all-to-all-done = bf16[32,2,512]{2,1,0:T(2,128)(2,1)S(1)} async-done(((bf16[32,2,512]{2,1,0:T(2,128)(2,1)}), bf16[32,2,512]{2,1,0:T(2,128)(2,1)S(1)}, u32[]{:S(2)}, u32[]{:S(2)}) %all-to-all-start) | async-done | bytes 65568 | tf_op jit(solution)/shard_map/all_to_all | solution.py:107
  75.4 3.5 %fusion.103 = f32[4,16,1024]{2,1,0:T(8,128)S(1)} fusion(bf16[4,16,512]{2,1,0:T(8,128)(2,1)S(1)} %all_to_all.58, bf16[4,1024,512]{2,1,0:T(8,128)(2,1)} %param.28), kind=kOutput, calls=%fused_computation.145 | convolution fusion | flops 67108864 | bytes 4521984 | tf_op jit(solution)/shard_map/bhr,blr->bhl/dot_general | solution.py:115
  80.9 3.3 %all-to-all-start.3 = ((bf16[4,16,512]{2,0,1:T(4,128)(2,1)}), bf16[4,16,512]{2,0,1:T(4,128)(2,1)S(1)}, u32[]{:S(2)}, u32[]{:S(2)}) async-start(bf16[4,16,512]{2,0,1:T(4,128)(2,1)} %copy.68), calls=%async_computation.3 | async-start | bytes 131072 | tf_op jit(solution)/shard_map/all_to_all | solution.py:147
  85.1 5.1 %all-to-all-done.3 = bf16[4,16,512]{2,0,1:T(4,128)(2,1)S(1)} async-done(((bf16[4,16,512]{2,0,1:T(4,128)(2,1)}), bf16[4,16,512]{2,0,1:T(4,128)(2,1)S(1)}, u32[]{:S(2)}, u32[]{:S(2)}) %all-to-all-start.3) | async-done | bytes 65568 | tf_op jit(solution)/shard_map/all_to_all | solution.py:147
  90.2 1.3 convolution_bitcast_fusion
  92.3 54.0 %all-reduce.4.cloned.1.call-done = bf16[32,2048]{1,0:T(8,128)(2,1)} async-done(((bf16[32,2048]{1,0:T(8,128)(2,1)}), bf16[32,2048]{1,0:T(8,128)(2,1)}) %all-reduce.4.cloned.1.call-update) | async-done | bytes 131088 | tf_op jit(solution)/shard_map/psum | solution.py:160
  147.4 1.8 fusion.2
  149.2 3.6 %all-to-all-start.4 = ((bf16[4,1,8,2048]{3,2,1,0:T(8,128)(2,1)}), bf16[4,1,8,2048]{3,2,1,0:T(8,128)(2,1)S(1)}, u32[]{:S(2)}, u32[]{:S(2)}) async-start(bf16[4,1,8,2048]{3,2,1,0:T(8,128)(2,1)} %fusion.2), calls=%async_computation.4 | async-start | bytes 262144 | tf_op jit(solution)/shard_map/all_to_all | solution.py:195
  152.9 1.8 fusion.99
  154.6 1.9 fusion.100
  156.5 1.4 all-to-all-done.4
  157.9 2.0 fusion.13
  160.0 3.2 %fusion.3 = bf16[4,1,8,2048]{3,2,1,0:T(8,128)(2,1)} fusion(bf16[1,512,2048]{2,1,0:T(8,128)(2,1)S(1)} %copy-done, bf16[1,2048,512]{2,1,0:T(8,128)(2,1)} %param.43, bf16[4,1,8,2048]{3,2,1,0:T(8,128)(2,1)S(1)} %all-to-all-done.4, f32[4,1,8,512]{3,2,0,1:T(8,128)S(1)} %fusion.13), kind=kOutput, calls=%fused_computation.8 | convolution fusion | flops 134381568 | bytes 4521984 | tf_op jit(solution)/shard_map/sxcf,xfd->sxcd/dot_general | solution.py:201
  163.2 3.5 %all-to-all-start.5 = ((bf16[4,1,8,2048]{3,2,1,0:T(8,128)(2,1)}), bf16[4,1,8,2048]{3,2,1,0:T(8,128)(2,1)S(1)}, u32[]{:S(2)}, u32[]{:S(2)}) async-start(bf16[4,1,8,2048]{3,2,1,0:T(8,128)(2,1)} %fusion.3), calls=%async_computation.5 | async-start | bytes 262144 | tf_op jit(solution)/shard_map/all_to_all | solution.py:204
  167.4 4.2 %all-to-all-done.5 = bf16[4,1,8,2048]{3,2,1,0:T(8,128)(2,1)S(1)} async-done(((bf16[4,1,8,2048]{3,2,1,0:T(8,128)(2,1)}), bf16[4,1,8,2048]{3,2,1,0:T(8,128)(2,1)S(1)}, u32[]{:S(2)}, u32[]{:S(2)}) %all-to-all-start.5) | async-done | bytes 131104 | tf_op jit(solution)/shard_map/all_to_all | solution.py:204
  171.9 1.4 convolution_add_fusion
  173.3 2.2 fusion.1
  176.8 51.4 %all-reduce.6.cloned.1.call-done = bf16[32,2048]{1,0:T(8,128)(2,1)} async-done(((bf16[32,2048]{1,0:T(8,128)(2,1)}), bf16[32,2048]{1,0:T(8,128)(2,1)}) %all-reduce.6.cloned.1.call-update) | async-done | bytes 131088
  228.2 1.4 add_convert_fusion
  (107 shorter events, 21.0 us)
Async XLA Ops:
  7.2 152.8 %copy-start = (bf16[1,512,2048]{2,1,0:T(8,128)(2,1)S(1)}, bf16[1,512,2048]{2,1,0:T(8,128)(2,1)}, u32[]{:S(2)}) copy-start(bf16[1,512,2048]{2,1,0:T(8,128)(2,1)} %param.44) | copy-start | bytes 6291460
  7.2 40.2 %copy-start.3 = (bf16[2048,2,64]{0,2,1:T(8,128)(2,1)S(1)}, bf16[2048,2,64]{0,2,1:T(8,128)(2,1)}, u32[]{:S(2)}) copy-start(bf16[2048,2,64]{0,2,1:T(8,128)(2,1)} %param.33) | copy-start | bytes 1572868
  7.2 44.6 %copy-start.11 = (bf16[512,2,64]{0,2,1:T(8,128)(2,1)S(1)}, bf16[512,2,64]{0,2,1:T(8,128)(2,1)}, u32[]{:S(2)}) copy-start(bf16[512,2,64]{0,2,1:T(8,128)(2,1)} %param.38) | copy-start | bytes 393220
  7.2 62.2 %copy-start.16 = (f32[512]{0:T(512)S(1)}, f32[512]{0:T(512)}, u32[]{:S(2)}) copy-start(f32[512]{0:T(512)} %param.37) | copy-start | bytes 6148
  9.0 6.0 %collective-permute-start = (bf16[4,2048]{1,0:T(4,128)(2,1)S(1)}, bf16[4,2048]{1,0:T(4,128)(2,1)S(1)}, u32[]{:S(2)}, u32[]{:S(2)}) collective-permute-start(bf16[4,2048]{1,0:T(4,128)(2,1)S(1)} %fusion.63), channel_id=1, source_target_pairs={{0,1},{1,2},{2,3},{3,4},{4,5},{5,6},{6,7},{7,0},{8,9},{9,10},{10,1... | collective-permute-start | bytes 49160 | tf_op jit(solution)/shard_map/ppermute | solution.py:84
  15.0 5.0 %collective-permute-start.1 = (bf16[4,2048]{1,0:T(4,128)(2,1)S(1)}, bf16[4,2048]{1,0:T(4,128)(2,1)S(1)}, u32[]{:S(2)}, u32[]{:S(2)}) collective-permute-start(bf16[4,2048]{1,0:T(4,128)(2,1)S(1)} %collective-permute-done), channel_id=1, source_target_pairs={{0,1},{1,2},{2,3},{3,4},{4,5},{5,6},{6,7},{7,0},{8,9},{9,10},{10,1... | collective-permute-start | bytes 49160 | tf_op jit(solution)/shard_map/ppermute | solution.py:84
  20.0 5.0 %collective-permute-start.2 = (bf16[4,2048]{1,0:T(4,128)(2,1)S(1)}, bf16[4,2048]{1,0:T(4,128)(2,1)S(1)}, u32[]{:S(2)}, u32[]{:S(2)}) collective-permute-start(bf16[4,2048]{1,0:T(4,128)(2,1)S(1)} %collective-permute-done.1), channel_id=1, source_target_pairs={{0,1},{1,2},{2,3},{3,4},{4,5},{5,6},{6,7},{7,0},{8,9},{9,10},{10,1... | collective-permute-start | bytes 49160 | tf_op jit(solution)/shard_map/ppermute | solution.py:84
  24.9 5.0 %collective-permute-start.3 = (bf16[4,2048]{1,0:T(4,128)(2,1)S(1)}, bf16[4,2048]{1,0:T(4,128)(2,1)S(1)}, u32[]{:S(2)}, u32[]{:S(2)}) collective-permute-start(bf16[4,2048]{1,0:T(4,128)(2,1)S(1)} %collective-permute-done.2), channel_id=1, source_target_pairs={{0,1},{1,2},{2,3},{3,4},{4,5},{5,6},{6,7},{7,0},{8,9},{9,10},{10,1... | collective-permute-start | bytes 49160 | tf_op jit(solution)/shard_map/ppermute | solution.py:84
  29.9 5.0 %collective-permute-start.4 = (bf16[4,2048]{1,0:T(4,128)(2,1)S(1)}, bf16[4,2048]{1,0:T(4,128)(2,1)S(1)}, u32[]{:S(2)}, u32[]{:S(2)}) collective-permute-start(bf16[4,2048]{1,0:T(4,128)(2,1)S(1)} %collective-permute-done.3), channel_id=1, source_target_pairs={{0,1},{1,2},{2,3},{3,4},{4,5},{5,6},{6,7},{7,0},{8,9},{9,10},{10,1... | collective-permute-start | bytes 49160 | tf_op jit(solution)/shard_map/ppermute | solution.py:84
  30.0 18.4 %copy-start.13 = (bf16[4,16]{1,0:T(4,128)(2,1)}, bf16[4,16]{1,0:T(4,128)(2,1)S(1)}, u32[]{:S(2)}) copy-start(bf16[4,16]{1,0:T(4,128)(2,1)S(1)} %get-tuple-element.10) | copy-start | bytes 388
  34.9 5.0 %collective-permute-start.5 = (bf16[4,2048]{1,0:T(4,128)(2,1)S(1)}, bf16[4,2048]{1,0:T(4,128)(2,1)S(1)}, u32[]{:S(2)}, u32[]{:S(2)}) collective-permute-start(bf16[4,2048]{1,0:T(4,128)(2,1)S(1)} %collective-permute-done.4), channel_id=1, source_target_pairs={{0,1},{1,2},{2,3},{3,4},{4,5},{5,6},{6,7},{7,0},{8,9},{9,10},{10,1... | collective-permute-start | bytes 49160 | tf_op jit(solution)/shard_map/ppermute | solution.py:84
  39.8 5.0 %collective-permute-start.6 = (bf16[4,2048]{1,0:T(4,128)(2,1)S(1)}, bf16[4,2048]{1,0:T(4,128)(2,1)S(1)}, u32[]{:S(2)}, u32[]{:S(2)}) collective-permute-start(bf16[4,2048]{1,0:T(4,128)(2,1)S(1)} %collective-permute-done.5), channel_id=1, source_target_pairs={{0,1},{1,2},{2,3},{3,4},{4,5},{5,6},{6,7},{7,0},{8,9},{9,10},{10,1... | collective-permute-start | bytes 49160 | tf_op jit(solution)/shard_map/ppermute | solution.py:84
  48.4 8.8 %all-to-all-start.2 = ((bf16[8,2,128]{2,1,0:T(2,128)(2,1)}), bf16[8,2,128]{2,1,0:T(2,128)(2,1)S(1)}, u32[]{:S(2)}, u32[]{:S(2)}) async-start(bf16[8,2,128]{2,1,0:T(2,128)(2,1)} %reshape.222), calls=%async_computation.2 | async-start | bytes 8192 | tf_op jit(solution)/shard_map/all_to_all | solution.py:109
  57.2 8.8 %all-to-all-start.1 = ((bf16[8,2,128]{2,1,0:T(2,128)(2,1)}), bf16[8,2,128]{2,1,0:T(2,128)(2,1)S(1)}, u32[]{:S(2)}, u32[]{:S(2)}) async-start(bf16[8,2,128]{2,1,0:T(2,128)(2,1)} %reshape.220), calls=%async_computation.1 | async-start | bytes 8192 | tf_op jit(solution)/shard_map/all_to_all | solution.py:108
  66.0 9.2 %all-to-all-start = ((bf16[32,2,512]{2,1,0:T(2,128)(2,1)}), bf16[32,2,512]{2,1,0:T(2,128)(2,1)S(1)}, u32[]{:S(2)}, u32[]{:S(2)}) async-start(bf16[32,2,512]{2,1,0:T(2,128)(2,1)} %copy.64), calls=%async_computation | async-start | bytes 131072 | tf_op jit(solution)/shard_map/all_to_all | solution.py:107
  69.5 9.4 %copy-start.15 = (bf16[4,512]{1,0:T(4,128)(2,1)}, bf16[4,512]{1,0:T(4,128)(2,1)S(1)}, u32[]{:S(2)}) copy-start(bf16[4,512]{1,0:T(4,128)(2,1)S(1)} %get-tuple-element.4) | copy-start | bytes 12292
  75.4 4.1 %copy-start.1 = (bf16[4,1024,512]{2,1,0:T(8,128)(2,1)S(1)}, bf16[4,1024,512]{2,1,0:T(8,128)(2,1)}, u32[]{:S(2)}) copy-start(bf16[4,1024,512]{2,1,0:T(8,128)(2,1)} %param.28) | copy-start | bytes 12582916
  79.5 4.8 %copy-start.17 = (f32[32,4]{0,1:T(4,128)S(1)}, f32[32,4]{0,1:T(4,128)}, u32[]{:S(2)}) copy-start(f32[32,4]{0,1:T(4,128)} %param.31) | copy-start | bytes 1540
  79.5 10.7 %copy-start.5 = (bf16[2,64,2048]{2,1,0:T(8,128)(2,1)S(1)}, bf16[2,64,2048]{2,1,0:T(8,128)(2,1)}, u32[]{:S(2)}) copy-start(bf16[2,64,2048]{2,1,0:T(8,128)(2,1)} %param.40) | copy-start | bytes 1572868
  79.5 12.0 %copy-start.10 = (bf16[4,2048]{1,0:T(4,128)(2,1)S(1)}, bf16[4,2048]{1,0:T(4,128)(2,1)}, u32[]{:S(2)}) copy-start(bf16[4,2048]{1,0:T(4,128)(2,1)} %param.26) | copy-start | bytes 49156
  80.3 67.1 %copy-start.9 = (f32[2048]{0:T(1024)S(1)}, f32[2048]{0:T(1024)}, u32[]{:S(2)}) copy-start(f32[2048]{0:T(1024)} %param.41) | copy-start | bytes 24580
  80.3 72.6 %copy-start.4 = (bf16[2048,128]{1,0:T(8,128)(2,1)S(1)}, bf16[2048,128]{1,0:T(8,128)(2,1)}, u32[]{:S(2)}) copy-start(bf16[2048,128]{1,0:T(8,128)(2,1)} %param.48) | copy-start | bytes 1572868
  80.9 9.2 %all-to-all-start.3 = ((bf16[4,16,512]{2,0,1:T(4,128)(2,1)}), bf16[4,16,512]{2,0,1:T(4,128)(2,1)S(1)}, u32[]{:S(2)}, u32[]{:S(2)}) async-start(bf16[4,16,512]{2,0,1:T(4,128)(2,1)} %copy.68), calls=%async_computation.3 | async-start | bytes 131072 | tf_op jit(solution)/shard_map/all_to_all | solution.py:147
  84.3 62.1 %all-reduce.4.cloned.1.call-start = ((), (), s32[]{:S(2)}) async-start(), calls=%async_computation.6 | async-start | bytes 262144 | tf_op jit(solution)/shard_map/psum | solution.py:160
  149.2 8.7 %all-to-all-start.4 = ((bf16[4,1,8,2048]{3,2,1,0:T(8,128)(2,1)}), bf16[4,1,8,2048]{3,2,1,0:T(8,128)(2,1)S(1)}, u32[]{:S(2)}, u32[]{:S(2)}) async-start(bf16[4,1,8,2048]{3,2,1,0:T(8,128)(2,1)} %fusion.2), calls=%async_computation.4 | async-start | bytes 262144 | tf_op jit(solution)/shard_map/all_to_all | solution.py:195
  159.9 6.7 %copy-start.2 = (bf16[32,2048]{1,0:T(8,128)(2,1)S(1)}, bf16[32,2048]{1,0:T(8,128)(2,1)}, u32[]{:S(2)}) copy-start(bf16[32,2048]{1,0:T(8,128)(2,1)} %all-reduce.4.cloned.1.call-done) | copy-start | bytes 393220
  159.9 6.7 %copy-start.14 = (bf16[2048,1]{0,1:T(2,128)(2,1)S(1)}, bf16[2048,1]{0,1:T(2,128)(2,1)}, u32[]{:S(2)}) copy-start(bf16[2048,1]{0,1:T(2,128)(2,1)} %reshape.217) | copy-start | bytes 12292
  159.9 11.7 %copy-start.12 = (f32[32,32]{1,0:T(8,128)S(1)}, f32[32,32]{1,0:T(8,128)}, u32[]{:S(2)}) copy-start(f32[32,32]{1,0:T(8,128)} %select_reduce_fusion) | copy-start | bytes 12292
  160.0 11.9 %copy-start.8 = (bf16[64,2048]{1,0:T(8,128)(2,1)S(1)}, bf16[64,2048]{1,0:T(8,128)(2,1)}, u32[]{:S(2)}) copy-start(bf16[64,2048]{1,0:T(8,128)(2,1)} %param.47) | copy-start | bytes 786436
  163.2 10.2 %copy-start.6 = (bf16[128,2048]{1,0:T(8,128)(2,1)S(1)}, bf16[128,2048]{1,0:T(8,128)(2,1)}, u32[]{:S(2)}) copy-start(bf16[128,2048]{1,0:T(8,128)(2,1)} %param.50) | copy-start | bytes 1572868
  163.2 8.4 %all-to-all-start.5 = ((bf16[4,1,8,2048]{3,2,1,0:T(8,128)(2,1)}), bf16[4,1,8,2048]{3,2,1,0:T(8,128)(2,1)S(1)}, u32[]{:S(2)}, u32[]{:S(2)}) async-start(bf16[4,1,8,2048]{3,2,1,0:T(8,128)(2,1)} %fusion.3), calls=%async_computation.5 | async-start | bytes 262144 | tf_op jit(solution)/shard_map/all_to_all | solution.py:204
  166.6 61.6 %all-reduce.6.cloned.1.call-start = ((), (), s32[]{:S(2)}) async-start(), calls=%async_computation.7 | async-start | bytes 262144
  (1 other events, 3.5 us)
Sparse Core Ops, SparseCore 0:
  92.4 53.9 all-reduce.3
  175.6 52.5 all-reduce.5
